TPU v7x, 256 devices: a whole 4x4x8 slice. The times are simulated.
256 devices in a mesh: sp: 32 (over z, x), tp: 8 (over y, core).
Axes of the slice: x: 4, y: 4, z: 8, core: 2. Of those that a mesh axis runs over, the one named last changes fastest.
Arguments:
- tokens: bfloat16 [24576, 4096], P('sp', 'tp'), may hold values from -6 to 6
- norm_gain: float32 [4096], replicated, may hold values from 0.1 to 1.9
- w_query: bfloat16 [4096, 2048], P('sp', 'tp'), may hold values from -0.09375 to 0.09375
- w_key: bfloat16 [4096, 1024], P('sp', 'tp'), may hold values from -0.09375 to 0.09375
- w_value: bfloat16 [4096, 1024], P('sp', 'tp'), may hold values from -0.09375 to 0.09375
- w_pool: bfloat16 [4096, 1024], P('sp', 'tp'), may hold values from -0.09375 to 0.09375
- query_gain: float32 [64], replicated, may hold values from 0.5 to 8
- key_gain: float32 [64], replicated, may hold values from 0.5 to 8
- sink_logit: float32 [32], P('tp'), may hold values from 1 to 5
- w_out_pool: bfloat16 [1024, 4096], P('tp', 'sp'), may hold values from -0.75 to 0.75
- w_out_attn: bfloat16 [2048, 4096], P('tp', 'sp'), may hold values from -1.5 to 1.5
Outputs:
- mixed: bfloat16 [24576, 4096], P(('sp', 'tp'))
All inputs are finite; a program needn't handle non-finite values.
Results may differ from a plain program's by a relative error of at most 0.014.
The roundings to bfloat16 on the way count: a program that leaves them out, or rounds other values in their place, can miss the bound.
Values may be sent and summed in bfloat16 or wider, within the bound.
No kernel may reach another device: no remote copies, remote signals or barrier semaphores. Data moves between devices by JAX's collectives and lax.ppermute only.
A program may use at most 128 MiB of HBM per device.

v0:
```python
import jax
import jax.numpy as jnp
from jax import lax
from jax.sharding import PartitionSpec as P

HEAD = 64
POOL = 1024
WINDOW = 128
GRID_W = 64
eps = 1e-06
rope_base = 10000.0
neg_big = -1e30
pool_reach = 8


def padded_2(block, sides, width):
    for axis, dim in sides:
        count = lax.axis_size(axis)
        forward = [(i, i + 1) for i in range(count - 1)]
        backward = [(target, source) for source, target in forward]
        low = lax.ppermute(
            lax.slice_in_dim(block, block.shape[dim] - width, None, axis=dim), axis, forward
        )
        high = lax.ppermute(lax.slice_in_dim(block, 0, width, axis=dim), axis, backward)
        block = jnp.concatenate([low, block, high], axis=dim)
    return block


def sent_together(arrays, axis, dim, along):
    ends, at = ([], 0)
    for a in arrays[:-1]:
        at += a.shape[along]
        ends.append(at)
    both = jnp.concatenate(arrays, axis=along)
    return tuple(jnp.split(lax.all_gather(both, axis, axis=dim, tiled=True), ends, axis=along))


def rope_tables(positions, head_size):
    quarter = head_size // 4
    freqs = 1.0 / rope_base ** (jnp.arange(quarter, dtype=jnp.float32) * 2.0 / (head_size // 2))
    row_angle = (positions // GRID_W).astype(jnp.float32)[:, None] * freqs
    col_angle = (positions % GRID_W).astype(jnp.float32)[:, None] * freqs
    angles = jnp.concatenate([row_angle, row_angle, col_angle, col_angle], axis=-1)
    return (jnp.cos(angles), jnp.sin(angles))


def rotate(heads_in, cosine, sine):
    part_one, part_two, part_three, part_four = jnp.split(heads_in, 4, axis=-1)
    turned = jnp.concatenate([-part_two, part_one, -part_four, part_three], axis=-1)
    return heads_in * cosine[:, None, :] + turned * sine[:, None, :]


def prepare(projected, gain, cosine, sine):
    rows_count = projected.shape[0]
    shaped = projected.reshape(rows_count, -1, HEAD)
    scaled = shaped * lax.rsqrt(jnp.mean(shaped * shaped, axis=-1, keepdims=True) + eps) * gain
    return rotate(scaled, cosine, sine).reshape(rows_count, -1).astype(jnp.bfloat16)


def edge_keys(keys_new, values_new):
    joined = jnp.concatenate([keys_new, values_new], axis=1)
    return padded_2(joined, (("sp", 0),), WINDOW)


def edge_pool(pool_in):
    return padded_2(pool_in, (("sp", 0),), pool_reach)


def window_attention(queries, key_band, sink_logit, positions, seq):
    rows_count = queries.shape[0]
    key_width = key_band.shape[1] // 2
    heads_q = queries.shape[1] // HEAD
    heads_k = key_width // HEAD
    group = heads_q // heads_k
    blocks = rows_count // WINDOW
    stacked = key_band.reshape(blocks + 2, WINDOW, 2 * key_width)
    joined = jnp.concatenate([stacked[:-2], stacked[1:-1], stacked[2:]], axis=1)
    block_keys = joined[:, :, :key_width].reshape(blocks, 3 * WINDOW, heads_k, HEAD)
    block_values = joined[:, :, key_width:].reshape(blocks, 3 * WINDOW, heads_k, HEAD)
    block_queries = queries.reshape(blocks, WINDOW, heads_k, group, HEAD)
    scores = jnp.einsum(
        "nqhgd,nkhd->nhgqk", block_queries, block_keys, preferred_element_type=jnp.float32
    ) * HEAD ** (-0.5)
    query_pos = positions.reshape(blocks, WINDOW)
    key_pos = query_pos[:, :1] - WINDOW + jnp.arange(3 * WINDOW, dtype=jnp.int32)[None, :]
    inside = (
        (jnp.abs(query_pos[:, :, None] - key_pos[:, None, :]) <= WINDOW)
        & (key_pos[:, None, :] >= 0)
        & (key_pos[:, None, :] < seq)
    )
    scores = jnp.where(inside[:, None, None], scores, neg_big)
    sink = sink_logit.reshape(heads_k, group)[None, :, :, None, None]
    top = jnp.maximum(jnp.max(scores, axis=-1, keepdims=True), sink)
    raised = jnp.exp(scores - top)
    totals = jnp.sum(raised, axis=-1, keepdims=True) + jnp.exp(sink - top)
    weights = (raised / totals).astype(jnp.bfloat16)
    result = jnp.einsum(
        "nhgqk,nkhd->nqhgd", weights, block_values, preferred_element_type=jnp.float32
    )
    return result.astype(jnp.bfloat16).reshape(rows_count, heads_q * HEAD)


def window_pool(pool_band, pool_in, positions, seq):
    rows_count = pool_in.shape[0]
    level = lax.axis_index("tp") * pool_in.shape[1] // (POOL // 4)
    padded = pool_band.astype(jnp.float32)
    sum_two = padded[:-1] + padded[1:]
    sum_four = sum_two[:-2] + sum_two[2:]
    sum_eight = sum_four[:-4] + sum_four[4:]
    sum_sixteen = sum_eight[:-8] + sum_eight[8:]
    candidates = jnp.stack(
        [
            sum_two[7 : 7 + rows_count],
            sum_four[6 : 6 + rows_count],
            sum_eight[4 : 4 + rows_count],
            sum_sixteen[:rows_count],
        ]
    )
    chosen = lax.dynamic_index_in_dim(candidates, level, 0, keepdims=False)
    reach = jnp.left_shift(jnp.int32(1), level)
    low = jnp.clip(positions - reach, 0, seq - 1)
    high = jnp.clip(positions + reach - 1, 0, seq - 1)
    counted = (high - low + 1).astype(jnp.float32)
    return (chosen / counted[:, None]).astype(jnp.bfloat16)


def shards(
    tokens,
    norm_gain,
    w_query,
    w_key,
    w_value,
    w_pool,
    query_gain,
    key_gain,
    sink_logit,
    w_out_pool,
    w_out_attn,
):
    gathered = lax.all_gather(tokens, "tp", axis=1, tiled=True)
    rows_count = gathered.shape[0]
    widened = gathered.astype(jnp.float32)
    normed = (
        widened * lax.rsqrt(jnp.mean(widened * widened, axis=1, keepdims=True) + eps) * norm_gain
    ).astype(jnp.bfloat16)
    positions = lax.axis_index("sp") * rows_count + jnp.arange(rows_count, dtype=jnp.int32)
    seq = lax.axis_size("sp") * rows_count
    cosine, sine = rope_tables(positions, HEAD)
    pieces = sent_together((w_query, w_key, w_value, w_pool), "sp", 0, 1)
    query_raw, key_raw, value_raw, pool_raw = tuple(
        (jnp.dot(normed, piece, preferred_element_type=jnp.float32) for piece in pieces)
    )
    queries = prepare(query_raw, query_gain, cosine, sine)
    keys_new = prepare(key_raw, key_gain, cosine, sine)
    pool_in = pool_raw.astype(jnp.bfloat16)
    key_band = edge_keys(keys_new, value_raw.astype(jnp.bfloat16))
    pool_band = edge_pool(pool_in)
    pooled = window_pool(pool_band, pool_in, positions, seq)
    attended = window_attention(queries, key_band, sink_logit, positions, seq)
    out_pool, out_attn = sent_together((w_out_pool, w_out_attn), "sp", 1, 0)
    return lax.psum_scatter(
        (
            jnp.dot(pooled, out_pool, preferred_element_type=jnp.float32)
            + jnp.dot(attended, out_attn, preferred_element_type=jnp.float32)
        ).astype(jnp.bfloat16),
        "tp",
        scatter_dimension=0,
        tiled=True,
    )


def solution(mesh):
    placed = (
        P("sp", "tp"),
        P(),
        P("sp", "tp"),
        P("sp", "tp"),
        P("sp", "tp"),
        P("sp", "tp"),
        P(),
        P(),
        P("tp"),
        P("tp", "sp"),
        P("tp", "sp"),
    )
    return jax.shard_map(
        shards, mesh=mesh, in_specs=placed, out_specs=P(("sp", "tp"), None), check_vma=False
    )
```

profile of v0, /device:TPU:1, one launch (start us, length us, event | category | flops | bytes accessed | tf_op | source)
XLA Modules:
  0.0 294.5 jit_solution(10621798535016886993)
XLA Ops:
  6.5 0.7 all-gather.4.cloned.1.call-update
  7.3 1.6 pad_maximum_fusion.7
  9.0 1.5 pad_maximum_fusion.8
  10.9 0.7 max.27
  11.6 0.7 mul.195
  12.3 0.7 mul.217
  13.5 1.4 fusion.12
  14.9 41.9 %all-gather.4.cloned.1.call-done = bf16[768,4096]{1,0:T(8,128)(2,1)} async-done(((bf16[768,512]{1,0:T(8,128)(2,1)}), bf16[768,4096]{1,0:T(8,128)(2,1)}) %all-gather.4.cloned.1.call-update) | async-done | bytes 6291472 | tf_op jit(solution)/shard_map/all_gather | solution.py:140
  56.8 4.2 %fusion = f32[768]{0:T(1024)S(1)} fusion(bf16[768,4096]{1,0:T(8,128)(2,1)} %all-gather.4.cloned.1.call-done), kind=kLoop, calls=%fused_computation.2 | loop fusion | flops 9436416 | bytes 6294528 | tf_op jit(solution)/shard_map/reduce_sum | solution.py:144
  61.1 0.4 copy-done.1
  61.4 5.4 %fusion.2 = bf16[768,4096]{1,0:T(8,128)(2,1)} fusion(bf16[768,4096]{1,0:T(8,128)(2,1)S(1)} %copy-done.1, f32[4096]{0:T(1024)S(1)} %copy-done.3, f32[768]{0:T(1024)S(1)} %add_rsqrt_fusion.2), kind=kLoop, calls=%fused_computation.4 | loop fusion | flops 12582912 | bytes 12602368 | tf_op jit(solution)/shard_map/convert_element_type | solution.py:145
  66.8 74.1 %all-gather.6.cloned.1.call-done = bf16[4096,640]{1,0:T(8,128)(2,1)} async-done(((bf16[128,640]{1,0:T(8,128)(2,1)}), bf16[4096,640]{1,0:T(8,128)(2,1)}) %all-gather.6.cloned.1.call-update) | async-done | bytes 5242896 | tf_op jit(solution)/shard_map/all_gather | solution.py:35
  140.8 5.0 %convolution_convert_fusion.1 = bf16[768,128]{1,0:T(8,128)(2,1)S(1)} fusion(bf16[768,4096]{1,0:T(8,128)(2,1)} %fusion.2, bf16[4096,640]{1,0:T(8,128)(2,1)} %all-gather.6.cloned.1.call-done), kind=kOutput, calls=%fused_computation.26 | convolution fusion | flops 805404672 | bytes 7536640 | tf_op jit(solution)/shard_map/dot_general | solution.py:151
  145.8 1.9 collective-permute-start
  147.7 1.6 collective-permute-start.1
  149.3 3.5 %multiply_reduce_fusion.1 = (f32[768,2]{0,1:T(2,128)S(1)}, f32[768,128]{0,1:T(8,128)S(1)}) fusion(bf16[768,4096]{1,0:T(8,128)(2,1)S(1)} %copy-done, bf16[4096,640]{1,0:T(8,128)(2,1)} %all-gather.6.cloned.1.call-done), kind=kOutput, calls=%fused_computation.74 | convolution fusion | flops 805501440 | bytes 7739392 | tf_op jit(solution)/shard_map/dot_general | solution.py:151
  153.2 2.2 convolution_convert_fusion
  155.4 4.0 %collective-permute-start.2 = (bf16[128,256]{0,1:T(8,128)(2,1)S(1)}, bf16[128,256]{0,1:T(8,128)(2,1)S(1)}, u32[]{:S(2)}, u32[]{:S(2)}) collective-permute-start(bf16[128,256]{0,1:T(8,128)(2,1)S(1)} %get-tuple-element.16), channel_id=1, source_target_pairs={{0,8},{8,16},{16,24},{24,32},{32,40},{40,48},{48,56},{56,64},{64,7... | collective-permute-start | bytes 196616 | tf_op jit(solution)/shard_map/ppermute | solution.py:21
  159.4 1.5 collective-permute-start.3
  160.9 2.0 multiply_reduce_fusion
  163.4 0.5 reshape.301
  164.3 54.8 %all-gather.8.cloned.1.call-done = bf16[384,4096]{1,0:T(8,128)(2,1)} async-done(((bf16[384,128]{1,0:T(8,128)(2,1)}), bf16[384,4096]{1,0:T(8,128)(2,1)}) %all-gather.8.cloned.1.call-update) | async-done | bytes 3145744 | tf_op jit(solution)/shard_map/all_gather | solution.py:35
  219.1 7.6 %fusion.16 = f32[768,4096]{1,0:T(8,128)} fusion(bf16[384,4096]{1,0:T(8,128)(2,1)} %all-gather.8.cloned.1.call-done, s32[]{:T(128)S(6)} %select_n.33, f32[1,768,128]{2,1,0:T(8,128)S(1)} %get-tuple-element.38, f32[1,768,128]{2,1,0:T(8,128)S(1)} %get-tuple-element.39, f32[1,768,128]{2,1,0:T(8,128)S(1)} %get-tuple-element.40, ...), kind=kOutput, calls=%fused_computation.30 | convolution fusion | flops 805797888 | bytes 15207428 | tf_op jit(solution)/shard_map/dot_general | solution.py:163
  228.3 1.0 fusion.4
  229.3 1.0 fusion.3
  230.5 1.4 fusion.10
  232.1 0.5 slice-done
  232.6 1.3 slice-done.1
  233.9 1.2 slice-done.2
  235.1 0.9 copy-done.2
  236.0 4.5 %add_convert_fusion = bf16[768,4096]{1,0:T(8,128)(2,1)} fusion(f32[768,4096]{1,0:T(8,128)S(1)} %bitcast.93, bf16[384,4096]{1,0:T(8,128)(2,1)S(1)} %copy-done.2, bf16[32,8,6,128]{3,2,1,0:T(8,128)(2,1)S(1)} %bitcast.95), kind=kOutput, calls=%fused_computation.5 | convolution fusion | flops 1616904192 | bytes 21495808 | tf_op jit(solution)/shard_map/dot_general | solution.py:164
  240.6 47.4 %reduce-scatter.2.cloned.1.call-done = bf16[96,4096]{1,0:T(8,128)(2,1)} async-done(((bf16[768,4096]{1,0:T(8,128)(2,1)}), bf16[96,4096]{1,0:T(8,128)(2,1)}) %reduce-scatter.2.cloned.1.call-update) | async-done | bytes 786448 | tf_op jit(solution)/shard_map/reduce_scatter | solution.py:161
  (72 shorter events, 4.3 us)
Async XLA Ops:
  6.5 54.5 %copy-start.3 = (f32[4096]{0:T(1024)S(1)}, f32[4096]{0:T(1024)}, u32[]{:S(2)}) copy-start(f32[4096]{0:T(1024)} %param.12) | copy-start | bytes 49156
  6.5 50.3 %all-gather.4.cloned.1.call-start = ((), (), s32[]{:S(2)}) async-start(), calls=%async_computation.1 | async-start | bytes 7077888 | tf_op jit(solution)/shard_map/all_gather | solution.py:140
  7.3 133.6 %all-gather.6.cloned.1.call-start = ((), (), s32[]{:S(2)}) async-start(), calls=%async_computation.2 | async-start | bytes 5406720 | tf_op jit(solution)/shard_map/all_gather | solution.py:35
  8.9 210.1 %all-gather.8.cloned.1.call-start = ((), (), s32[]{:S(2)}) async-start(), calls=%async_computation.3 | async-start | bytes 3244032 | tf_op jit(solution)/shard_map/all_gather | solution.py:35
  10.5 277.5 %reduce-scatter.2.cloned.1.call-start = ((), (), s32[]{:S(2)}) async-start(), calls=%async_computation.4 | async-start | bytes 7077888 | tf_op jit(solution)/shard_map/reduce_scatter | solution.py:161
  56.8 4.6 %copy-start.1 = (bf16[768,4096]{1,0:T(8,128)(2,1)S(1)}, bf16[768,4096]{1,0:T(8,128)(2,1)}, u32[]{:S(2)}) copy-start(bf16[768,4096]{1,0:T(8,128)(2,1)} %all-gather.4.cloned.1.call-done) | copy-start | bytes 18874372
  140.8 8.5 %copy-start = (bf16[768,4096]{1,0:T(8,128)(2,1)S(1)}, bf16[768,4096]{1,0:T(8,128)(2,1)}, u32[]{:S(2)}) copy-start(bf16[768,4096]{1,0:T(8,128)(2,1)} %fusion.2) | copy-start | bytes 18874372
  145.8 18.1 %collective-permute-start = (bf16[8,128]{1,0:T(8,128)(2,1)S(1)}, bf16[8,128]{1,0:T(8,128)(2,1)S(1)}, u32[]{:S(2)}, u32[]{:S(2)}) collective-permute-start(bf16[8,128]{1,0:T(8,128)(2,1)S(1)} %get-tuple-element.22), channel_id=1, source_target_pairs={{0,8},{8,16},{16,24},{24,32},{32,40},{40,48},{48,56},{56,64},{64,7... | collective-permute-start | bytes 6152 | tf_op jit(solution)/shard_map/ppermute | solution.py:21
  147.7 5.4 %slice-start.3 = ((s8[5242880]{0:T(1024)(128)(4,1)}), s8[4194304]{0:T(1024)(128)(4,1)S(1)}, s32[]{:S(2)}) async-start(s8[5242880]{0:T(1024)(128)(4,1)} %bitcast.99), calls=%async_computation.8 | async-start | bytes 8388608
  147.7 5.1 %copy-start.5 = (f32[64]{0:T(128)S(1)}, f32[64]{0:T(128)}, u32[]{:S(2)}) copy-start(f32[64]{0:T(128)} %param.18) | copy-start | bytes 772
  147.7 5.4 %slice-start.4 = ((s8[5242880]{0:T(1024)(128)(4,1)}), s8[1048576]{0:T(1024)(128)(4,1)S(1)}, s32[]{:S(2)}) async-start(s8[5242880]{0:T(1024)(128)(4,1)} %bitcast.99), calls=%async_computation.9 | async-start | bytes 2097152
  147.7 16.2 %collective-permute-start.1 = (bf16[8,128]{1,0:T(8,128)(2,1)S(1)}, bf16[8,128]{1,0:T(8,128)(2,1)S(1)}, u32[]{:S(2)}, u32[]{:S(2)}) collective-permute-start(bf16[8,128]{1,0:T(8,128)(2,1)S(1)} %get-tuple-element.23), channel_id=1, source_target_pairs={{8,0},{16,8},{24,16},{32,24},{40,32},{48,40},{56,48},{64,56},{72,6... | collective-permute-start | bytes 6152 | tf_op jit(solution)/shard_map/ppermute | solution.py:24
  155.4 71.3 %collective-permute-start.2 = (bf16[128,256]{0,1:T(8,128)(2,1)S(1)}, bf16[128,256]{0,1:T(8,128)(2,1)S(1)}, u32[]{:S(2)}, u32[]{:S(2)}) collective-permute-start(bf16[128,256]{0,1:T(8,128)(2,1)S(1)} %get-tuple-element.16), channel_id=1, source_target_pairs={{0,8},{8,16},{16,24},{24,32},{32,40},{40,48},{48,56},{56,64},{64,7... | collective-permute-start | bytes 196616 | tf_op jit(solution)/shard_map/ppermute | solution.py:21
  159.4 3.5 %copy-start.4 = (f32[64]{0:T(128)S(1)}, f32[64]{0:T(128)}, u32[]{:S(2)}) copy-start(f32[64]{0:T(128)} %param.17) | copy-start | bytes 772
  159.4 67.2 %collective-permute-start.3 = (bf16[128,256]{0,1:T(8,128)(2,1)S(1)}, bf16[128,256]{0,1:T(8,128)(2,1)S(1)}, u32[]{:S(2)}, u32[]{:S(2)}) collective-permute-start(bf16[128,256]{0,1:T(8,128)(2,1)S(1)} %get-tuple-element.17), channel_id=1, source_target_pairs={{8,0},{16,8},{24,16},{32,24},{40,32},{48,40},{56,48},{64,56},{72,6... | collective-permute-start | bytes 196616 | tf_op jit(solution)/shard_map/ppermute | solution.py:24
  230.4 2.2 slice-start
  230.5 3.5 %slice-start.1 = ((s8[12582912]{0:T(1024)(128)(4,1)}), s8[4194304]{0:T(1024)(128)(4,1)S(1)}, s32[]{:S(2)}) async-start(s8[12582912]{0:T(1024)(128)(4,1)} %bitcast.92), calls=%async_computation.6 | async-start | bytes 8388608
  230.5 4.6 %slice-start.2 = ((s8[12582912]{0:T(1024)(128)(4,1)}), s8[4194304]{0:T(1024)(128)(4,1)S(1)}, s32[]{:S(2)}) async-start(s8[12582912]{0:T(1024)(128)(4,1)} %bitcast.92), calls=%async_computation.7 | async-start | bytes 8388608
  230.5 5.5 %copy-start.2 = (bf16[384,4096]{1,0:T(8,128)(2,1)S(1)}, bf16[384,4096]{1,0:T(8,128)(2,1)}, u32[]{:S(2)}) copy-start(bf16[384,4096]{1,0:T(8,128)(2,1)} %all-gather.8.cloned.1.call-done) | copy-start | bytes 9437188
Sparse Core Ops, SparseCore 0:
  9.2 47.6 all-gather.3
  59.4 81.3 all-gather.5
  143.3 75.7 all-gather.7
  240.7 47.2 reduce-scatter.1
where the time goes:
time: 295 us
  waiting for transfers between devices  219 us (74%)
  matrix products  27.1 us (9%)
  other arithmetic  17.2 us (6%)
  between operations  13.6 us (5%)
  starting transfers between devices  9 us (3%)
  local copies, waits for them, and re-layouts  8.74 us (3%)
    all_gather x2, waiting for transfers between devices, sent_together(): lax.all_gather(both, axis, axis=dim, tiled=True)  129 us
    reduce_scatter x1, waiting for transfers between devices, shards(): lax.psum_scatter((jnp.dot(pooled, out_pool, preferred_element_type=jnp.fl...  47.4 us
    all_gather x1, waiting for transfers between devices, shards(): gathered = lax.all_gather(tokens, 'tp', axis=1, tiled=True)  41.9 us
    dot_general x4, matrix products, shards(): jnp.dot(normed, piece, preferred_element_type=jnp.float32)  12.7 us
    dot_general x1, matrix products, shards(): jnp.dot(pooled, out_pool, preferred_element_type=jnp.float32)  7.6 us
  transfers between devices with their start and end apart: 8, of which 4 were waited for; matrix products, arithmetic and copies ran while one was open for 13% of the time, Pallas kernels for 0%

commit v1 on v0

--- a/solution.py
+++ b/solution.py
@@ -11,6 +11,12 @@
 rope_base = 10000.0
 neg_big = -1e30
 pool_reach = 8
+
+
+def joined_along(tiles, dim):
+    dims = list(tiles.shape[1:])
+    dims[dim] *= tiles.shape[0]
+    return jnp.moveaxis(tiles, 0, dim).reshape(dims)
 
 
 def padded_2(block, sides, width):
@@ -137,7 +143,19 @@
     w_out_pool,
     w_out_attn,
 ):
-    gathered = lax.all_gather(tokens, "tp", axis=1, tiled=True)
+    size = lax.axis_size("tp")
+    pairs = [(i_2, (i_2 + 1) % size) for i_2 in range(size)]
+    back = [(b, a_2) for a_2, b in pairs]
+    lower, upper = ([], [])
+    for step in range(size - 1):
+        if step % 2 == 0:
+            lower.append(lax.ppermute(lower[-1] if lower else tokens, "tp", pairs))
+        else:
+            upper.append(lax.ppermute(upper[-1] if upper else tokens, "tp", back))
+    parts = jnp.stack([*lower[::-1], tokens, *upper])
+    shift = lax.axis_index("tp") - len(lower)
+    parts = parts[(jnp.arange(size) - shift) % size]
+    gathered = joined_along(parts, 1)
     rows_count = gathered.shape[0]
     widened = gathered.astype(jnp.float32)
     normed = (

time: 295 us -> 254 us (0.86)
  waiting for transfers between devices: 219 us -> 96.2 us
  local copies, waits for them, and re-layouts: 8.74 us -> 52.6 us
  starting transfers between devices: 9 us -> 29.9 us
  other arithmetic: 17.2 us -> 34 us
    all_gather x2, waiting for transfers between devices: 129 us -> 27.3 us  [sent_together(): lax.all_gather(both, axis, axis=dim, tiled=True)]
    all_gather x1 -> x0, waiting for transfers between devices: 41.9 us -> none  [shards(): gathered = lax.all_gather(tokens, 'tp', axis=1, tiled=True)]
    ppermute x0 -> x7, waiting for transfers between devices: none -> 21.4 us  [the longest x4 21.2 us: shards(): lower.append(lax.ppermute(lower[-1] if lower else tokens, 'tp', pairs))]
    ppermute x0 -> x7, starting transfers between devices: none -> 18.7 us  [the longest x4 10 us: shards(): lower.append(lax.ppermute(lower[-1] if lower else tokens, 'tp', pairs))]
    convert_element_type x0 -> x2, local copies, waits for them, and re-layouts: none -> 13.1 us  [the longest x1 12.7 us: shards(): widened = gathered.astype(jnp.float32)]
    unnamed x22 -> x51, local copies, waits for them, and re-layouts: 4.27 us -> 12.3 us
    mul x4 -> x2, local copies, waits for them, and re-layouts: 1.48 us -> 9.38 us  [shards(): widened * lax.rsqrt(jnp.mean(widened * widened, axis=1, keepdims=True) +...]
    dot_general x0 -> x4, local copies, waits for them, and re-layouts: none -> 7.62 us  [shards(): jnp.dot(normed, piece, preferred_element_type=jnp.float32)]
  transfers between devices with their start and end apart: 8 -> 14, of which waited for: 4 -> 7; matrix products, arithmetic and copies ran while one was open for 13% -> 37% of each run, Pallas kernels for 0% -> 0%
where the time goes in v1:
time: 254 us
  waiting for transfers between devices  96.2 us (38%)
  local copies, waits for them, and re-layouts  52.6 us (21%)
  other arithmetic  34 us (13%)
  starting transfers between devices  29.9 us (12%)
  matrix products  27.2 us (11%)
  between operations  13.6 us (5%)
    reduce_scatter x1, waiting for transfers between devices, shards(): lax.psum_scatter((jnp.dot(pooled, out_pool, preferred_element_type=jnp.fl...  47.5 us
    all_gather x2, waiting for transfers between devices, sent_together(): lax.all_gather(both, axis, axis=dim, tiled=True)  27.3 us
    ppermute x4, waiting for transfers between devices, shards(): lower.append(lax.ppermute(lower[-1] if lower else tokens, 'tp', pairs))  21.2 us
    convert_element_type x1, local copies, waits for them, and re-layouts, shards(): widened = gathered.astype(jnp.float32)  12.7 us
    unnamed x51, local copies, waits for them, and re-layouts  12.3 us
    dot_general x4, matrix products, shards(): jnp.dot(normed, piece, preferred_element_type=jnp.float32)  10.2 us
    ppermute x4, starting transfers between devices, shards(): lower.append(lax.ppermute(lower[-1] if lower else tokens, 'tp', pairs))  10 us
    mul x2, local copies, waits for them, and re-layouts, shards(): widened * lax.rsqrt(jnp.mean(widened * widened, axis=1, keepdims=True) +...  9.38 us
  transfers between devices with their start and end apart: 14, of which 7 were waited for; matrix products, arithmetic and copies ran while one was open for 37% of the time, Pallas kernels for 0%

profile of v1, /device:TPU:1, one launch (start us, length us, event | category | flops | bytes accessed | tf_op | source)
XLA Modules:
  0.0 253.6 jit_solution(12001963821651043041)
XLA Ops:
  6.5 1.6 pad_maximum_fusion.7
  8.3 2.7 %collective-permute-start = (bf16[768,512]{1,0:T(8,128)(2,1)}, bf16[768,512]{1,0:T(8,128)(2,1)S(1)}, u32[]{:S(2)}, u32[]{:S(2)}) collective-permute-start(bf16[768,512]{1,0:T(8,128)(2,1)} %param.11), channel_id=1, source_target_pairs={{0,1},{1,2},{2,3},{3,4},{4,5},{5,6},{6,7},{7,0},{8,9},{9,10},{10,1... | collective-permute-start | bytes 2359304 | tf_op jit(solution)/shard_map/ppermute | solution.py:152
  10.9 9.3 %collective-permute-done = bf16[768,512]{1,0:T(8,128)(2,1)S(1)} collective-permute-done((bf16[768,512]{1,0:T(8,128)(2,1)}, bf16[768,512]{1,0:T(8,128)(2,1)S(1)}, u32[]{:S(2)}, u32[]{:S(2)}) %collective-permute-start) | collective-permute-done | bytes 786464 | tf_op jit(solution)/shard_map/ppermute | solution.py:152
  20.2 2.4 collective-permute-start.1
  22.6 1.7 collective-permute-start.4
  27.4 4.1 %collective-permute-done.1 = bf16[768,512]{1,0:T(8,128)(2,1)S(1)} collective-permute-done((bf16[768,512]{1,0:T(8,128)(2,1)S(1)}, bf16[768,512]{1,0:T(8,128)(2,1)S(1)}, u32[]{:S(2)}, u32[]{:S(2)}) %collective-permute-start.1) | collective-permute-done | bytes 786464 | tf_op jit(solution)/shard_map/ppermute | solution.py:152
  31.5 2.5 collective-permute-start.2
  35.3 3.0 %collective-permute-start.5 = (bf16[768,512]{1,0:T(8,128)(2,1)S(1)}, bf16[768,512]{1,0:T(8,128)(2,1)S(1)}, u32[]{:S(2)}, u32[]{:S(2)}) collective-permute-start(bf16[768,512]{1,0:T(8,128)(2,1)S(1)} %collective-permute-done.4), channel_id=1, source_target_pairs={{1,0},{2,1},{3,2},{4,3},{5,4},{6,5},{7,6},{0,7},{9,8},{10,9},{11,1... | collective-permute-start | bytes 2359304 | tf_op jit(solution)/shard_map/ppermute | solution.py:154
  38.3 4.6 %collective-permute-done.2 = bf16[768,512]{1,0:T(8,128)(2,1)S(1)} collective-permute-done((bf16[768,512]{1,0:T(8,128)(2,1)S(1)}, bf16[768,512]{1,0:T(8,128)(2,1)S(1)}, u32[]{:S(2)}, u32[]{:S(2)}) %collective-permute-start.2) | collective-permute-done | bytes 786464 | tf_op jit(solution)/shard_map/ppermute | solution.py:152
  42.9 2.5 collective-permute-start.3
  47.2 4.0 %collective-permute-start.6 = (bf16[768,512]{1,0:T(8,128)(2,1)S(1)}, bf16[768,512]{1,0:T(8,128)(2,1)S(1)}, u32[]{:S(2)}, u32[]{:S(2)}) collective-permute-start(bf16[768,512]{1,0:T(8,128)(2,1)S(1)} %collective-permute-done.5), channel_id=1, source_target_pairs={{1,0},{2,1},{3,2},{4,3},{5,4},{6,5},{7,6},{0,7},{9,8},{10,9},{11,1... | collective-permute-start | bytes 2359304 | tf_op jit(solution)/shard_map/ppermute | solution.py:154
  51.1 3.2 %collective-permute-done.3 = bf16[768,512]{1,0:T(8,128)(2,1)S(1)} collective-permute-done((bf16[768,512]{1,0:T(8,128)(2,1)S(1)}, bf16[768,512]{1,0:T(8,128)(2,1)S(1)}, u32[]{:S(2)}, u32[]{:S(2)}) %collective-permute-start.3) | collective-permute-done | bytes 786464 | tf_op jit(solution)/shard_map/ppermute | solution.py:152
  61.9 6.7 %gather_fusion = bf16[8,768,512]{2,1,0:T(8,128)(2,1)} fusion(bf16[8,768,512]{2,1,0:T(8,128)(2,1)} %bitcast_dynamic-update-slice_fusion, s32[1024]{0:T(1024)S(1)} %pad_clamp_fusion), kind=kCustom, calls=%fused_computation | custom fusion | bytes 12582944 | tf_op jit(solution)/shard_map/gather | solution.py:157
  68.6 4.3 %fusion = f32[768]{0:T(1024)S(1)} fusion(bf16[8,768,512]{2,1,0:T(8,128)(2,1)} %gather_fusion), kind=kLoop, calls=%fused_computation.4 | loop fusion | flops 9436416 | bytes 6294528 | tf_op jit(solution)/shard_map/reduce_sum | solution.py:162
  73.4 6.3 %convert_bitcast_fusion = f32[768,8,512]{2,0,1:T(8,128)} fusion(bf16[8,768,512]{2,1,0:T(8,128)(2,1)S(1)} %copy-done), kind=kLoop, calls=%fused_computation.3 | loop fusion | flops 3145728 | bytes 18874368 | tf_op jit(solution)/shard_map/convert_element_type | solution.py:160
  79.8 4.6 %fusion.5 = bf16[768,8,512]{2,0,1:T(8,128)(2,1)} fusion(bf16[8,768,512]{2,1,0:T(8,128)(2,1)S(1)} %copy-done, f32[8,512]{1,0:T(8,128)S(1)} %mul.171, f32[768]{0:T(1024)S(1)} %add_rsqrt_fusion.2), kind=kLoop, calls=%fused_computation.11 | loop fusion | flops 12582912 | bytes 12602368 | tf_op jit(solution)/shard_map/mul | solution.py:162
  84.4 8.7 %copy.62 = bf16[768,8,512]{0,2,1:T(8,128)(2,1)} copy(bf16[768,8,512]{2,0,1:T(8,128)(2,1)} %fusion.5) | data formatting | bytes 12582912 | tf_op jit(solution)/shard_map/mul | solution.py:162
  93.0 12.7 %copy.61 = f32[768,8,512]{0,2,1:T(8,128)} copy(f32[768,8,512]{2,0,1:T(8,128)} %convert_bitcast_fusion) | data formatting | bytes 25165824 | tf_op jit(solution)/shard_map/convert_element_type | solution.py:160
  105.7 8.7 %fusion.4 = bf16[768,4096]{0,1:T(8,128)(2,1)} fusion(f32[768,8,512]{0,2,1:T(8,128)} %copy.61, f32[4096]{0:T(1024)S(1)} %copy-done.12, f32[768]{0:T(1024)S(1)} %add_rsqrt_fusion.2), kind=kLoop, calls=%fused_computation.9 | loop fusion | flops 9437184 | bytes 18893824 | tf_op jit(solution)/shard_map/convert_element_type | solution.py:163
  114.4 1.7 slice_bitcast_fusion
  116.2 3.1 %copy.70 = bf16[256,4096]{1,0:T(8,128)(2,1)} copy(bf16[256,4096]{0,1:T(8,128)(2,1)S(1)} %slice_bitcast_fusion) | data formatting | bytes 4194304 | tf_op jit(solution)/shard_map/dot_general | solution.py:169
  122.0 5.0 %convolution_convert_fusion.1 = bf16[768,128]{1,0:T(8,128)(2,1)S(1)} fusion(bf16[768,4096]{0,1:T(8,128)(2,1)} %fusion.4, bf16[4096,640]{1,0:T(8,128)(2,1)} %all-gather.3.cloned.1.call-done), kind=kOutput, calls=%fused_computation.31 | convolution fusion | flops 805404672 | bytes 7536640 | tf_op jit(solution)/shard_map/dot_general | solution.py:169
  127.1 3.1 %collective-permute-start.7 = (bf16[8,128]{1,0:T(8,128)(2,1)S(1)}, bf16[8,128]{1,0:T(8,128)(2,1)S(1)}, u32[]{:S(2)}, u32[]{:S(2)}) collective-permute-start(bf16[8,128]{1,0:T(8,128)(2,1)S(1)} %get-tuple-element.22), channel_id=1, source_target_pairs={{0,8},{8,16},{16,24},{24,32},{32,40},{40,48},{48,56},{56,64},{64,7... | collective-permute-start | bytes 6152 | tf_op jit(solution)/shard_map/ppermute | solution.py:27
  132.9 1.8 multiply_reduce_fusion
  135.9 2.3 convolution_convert_fusion
  140.7 5.2 %collective-permute-start.9 = (bf16[128,256]{0,1:T(8,128)(2,1)S(1)}, bf16[128,256]{0,1:T(8,128)(2,1)}, u32[]{:S(2)}, u32[]{:S(2)}) collective-permute-start(bf16[128,256]{0,1:T(8,128)(2,1)S(1)} %get-tuple-element.16), channel_id=1, source_target_pairs={{0,8},{8,16},{16,24},{24,32},{32,40},{40,48},{48,56},{56,64},{64,7... | collective-permute-start | bytes 196616 | tf_op jit(solution)/shard_map/ppermute | solution.py:27
  146.3 27.3 %all-gather.5.cloned.1.call-done = bf16[384,4096]{1,0:T(8,128)(2,1)} async-done(((bf16[384,128]{1,0:T(8,128)(2,1)}), bf16[384,4096]{1,0:T(8,128)(2,1)}) %all-gather.5.cloned.1.call-update) | async-done | bytes 3145744 | tf_op jit(solution)/shard_map/all_gather | solution.py:41
  173.6 7.6 %fusion.15 = f32[768,4096]{1,0:T(8,128)} fusion(bf16[384,4096]{1,0:T(8,128)(2,1)} %all-gather.5.cloned.1.call-done, s32[]{:T(128)S(6)} %select_n.58, f32[1,768,128]{2,1,0:T(8,128)S(1)} %get-tuple-element.38, f32[1,768,128]{2,1,0:T(8,128)S(1)} %get-tuple-element.39, f32[1,768,128]{2,1,0:T(8,128)S(1)} %get-tuple-element.40, ...), kind=kOutput, calls=%fused_computation.34 | convolution fusion | flops 805797888 | bytes 15207428 | tf_op jit(solution)/shard_map/dot_general | solution.py:181
  184.5 2.0 copy-done.1
  188.0 3.8 %fusion.11 = bf16[6,128,2,2,64]{1,4,3,2,0:T(8,128)(2,1)S(1)} fusion(bf16[6,384,2,64,1]{1,3,4,2,0:T(8,128)(2,1)S(1)} %bitcast.116, f32[6,2,384,128,2]{3,2,4,1,0:T(8,128)} %copy-done.1, f32[6,2,2,128]{3,2,1,0:T(2,128)S(1)} %exponential_add_fusion, f32[6,2,2,128]{3,2,1,0:T(2,128)S(1)} %broadcast_maximum_fusion, pred[6,128,384]{1,2,0:T(8,128)(4,1)S(1)} %fusion.13), kind=kOutput, calls=%fused_computation.25 | convolution fusion | flops 157089792 | bytes 6021120 | tf_op jit(solution)/shard_map/nhgqk,nkhd->nqhgd/dot_general | solution.py:103
  195.0 4.5 %add_convert_fusion = bf16[768,4096]{1,0:T(8,128)(2,1)} fusion(f32[768,4096]{1,0:T(8,128)S(1)} %bitcast.100, bf16[384,4096]{1,0:T(8,128)(2,1)S(1)} %copy-done.2, bf16[32,8,6,128]{3,2,1,0:T(8,128)(2,1)S(1)} %bitcast.111), kind=kOutput, calls=%fused_computation.10 | convolution fusion | flops 1616904192 | bytes 21495808 | tf_op jit(solution)/shard_map/dot_general | solution.py:182
  199.6 47.5 %reduce-scatter.2.cloned.1.call-done = bf16[96,4096]{1,0:T(8,128)(2,1)} async-done(((bf16[768,4096]{1,0:T(8,128)(2,1)}), bf16[96,4096]{1,0:T(8,128)(2,1)}) %reduce-scatter.2.cloned.1.call-update) | async-done | bytes 786448 | tf_op jit(solution)/shard_map/reduce_scatter | solution.py:179
  (120 shorter events, 31.2 us)
Async XLA Ops:
  6.5 51.6 %copy-start.7 = (bf16[768,512]{1,0:T(8,128)(2,1)S(1)}, bf16[768,512]{1,0:T(8,128)(2,1)}, u32[]{:S(2)}) copy-start(bf16[768,512]{1,0:T(8,128)(2,1)} %param.11) | copy-start | bytes 2359300
  6.5 107.9 %all-gather.3.cloned.1.call-start = ((), (), s32[]{:S(2)}) async-start(), calls=%async_computation.1 | async-start | bytes 5406720 | tf_op jit(solution)/shard_map/all_gather | solution.py:41
  8.2 165.4 %all-gather.5.cloned.1.call-start = ((), (), s32[]{:S(2)}) async-start(), calls=%async_computation.2 | async-start | bytes 3244032 | tf_op jit(solution)/shard_map/all_gather | solution.py:41
  8.3 11.9 %collective-permute-start = (bf16[768,512]{1,0:T(8,128)(2,1)}, bf16[768,512]{1,0:T(8,128)(2,1)S(1)}, u32[]{:S(2)}, u32[]{:S(2)}) collective-permute-start(bf16[768,512]{1,0:T(8,128)(2,1)} %param.11), channel_id=1, source_target_pairs={{0,1},{1,2},{2,3},{3,4},{4,5},{5,6},{6,7},{7,0},{8,9},{9,10},{10,1... | collective-permute-start | bytes 2359304 | tf_op jit(solution)/shard_map/ppermute | solution.py:152
  20.2 11.3 %collective-permute-start.1 = (bf16[768,512]{1,0:T(8,128)(2,1)S(1)}, bf16[768,512]{1,0:T(8,128)(2,1)S(1)}, u32[]{:S(2)}, u32[]{:S(2)}) collective-permute-start(bf16[768,512]{1,0:T(8,128)(2,1)S(1)} %collective-permute-done), channel_id=1, source_target_pairs={{0,1},{1,2},{2,3},{3,4},{4,5},{5,6},{6,7},{7,0},{8,9},{9,10},{10,1... | collective-permute-start | bytes 2359304 | tf_op jit(solution)/shard_map/ppermute | solution.py:152
  22.6 12.8 %collective-permute-start.4 = (bf16[768,512]{1,0:T(8,128)(2,1)}, bf16[768,512]{1,0:T(8,128)(2,1)S(1)}, u32[]{:S(2)}, u32[]{:S(2)}) collective-permute-start(bf16[768,512]{1,0:T(8,128)(2,1)} %param.11), channel_id=1, source_target_pairs={{1,0},{2,1},{3,2},{4,3},{5,4},{6,5},{7,6},{0,7},{9,8},{10,9},{11,1... | collective-permute-start | bytes 2359304 | tf_op jit(solution)/shard_map/ppermute | solution.py:154
  25.8 221.2 %reduce-scatter.2.cloned.1.call-start = ((), (), s32[]{:S(2)}) async-start(), calls=%async_computation.3 | async-start | bytes 7077888 | tf_op jit(solution)/shard_map/reduce_scatter | solution.py:179
  31.5 11.4 %collective-permute-start.2 = (bf16[768,512]{1,0:T(8,128)(2,1)S(1)}, bf16[768,512]{1,0:T(8,128)(2,1)S(1)}, u32[]{:S(2)}, u32[]{:S(2)}) collective-permute-start(bf16[768,512]{1,0:T(8,128)(2,1)S(1)} %collective-permute-done.1), channel_id=1, source_target_pairs={{0,1},{1,2},{2,3},{3,4},{4,5},{5,6},{6,7},{7,0},{8,9},{9,10},{10,1... | collective-permute-start | bytes 2359304 | tf_op jit(solution)/shard_map/ppermute | solution.py:152
  35.3 11.8 %collective-permute-start.5 = (bf16[768,512]{1,0:T(8,128)(2,1)S(1)}, bf16[768,512]{1,0:T(8,128)(2,1)S(1)}, u32[]{:S(2)}, u32[]{:S(2)}) collective-permute-start(bf16[768,512]{1,0:T(8,128)(2,1)S(1)} %collective-permute-done.4), channel_id=1, source_target_pairs={{1,0},{2,1},{3,2},{4,3},{5,4},{6,5},{7,6},{0,7},{9,8},{10,9},{11,1... | collective-permute-start | bytes 2359304 | tf_op jit(solution)/shard_map/ppermute | solution.py:154
  42.9 11.4 %collective-permute-start.3 = (bf16[768,512]{1,0:T(8,128)(2,1)S(1)}, bf16[768,512]{1,0:T(8,128)(2,1)S(1)}, u32[]{:S(2)}, u32[]{:S(2)}) collective-permute-start(bf16[768,512]{1,0:T(8,128)(2,1)S(1)} %collective-permute-done.2), channel_id=1, source_target_pairs={{0,1},{1,2},{2,3},{3,4},{4,5},{5,6},{6,7},{7,0},{8,9},{9,10},{10,1... | collective-permute-start | bytes 2359304 | tf_op jit(solution)/shard_map/ppermute | solution.py:152
  47.2 13.8 %collective-permute-start.6 = (bf16[768,512]{1,0:T(8,128)(2,1)S(1)}, bf16[768,512]{1,0:T(8,128)(2,1)S(1)}, u32[]{:S(2)}, u32[]{:S(2)}) collective-permute-start(bf16[768,512]{1,0:T(8,128)(2,1)S(1)} %collective-permute-done.5), channel_id=1, source_target_pairs={{1,0},{2,1},{3,2},{4,3},{5,4},{6,5},{7,6},{0,7},{9,8},{10,9},{11,1... | collective-permute-start | bytes 2359304 | tf_op jit(solution)/shard_map/ppermute | solution.py:154
  68.6 4.8 %copy-start = (bf16[8,768,512]{2,1,0:T(8,128)(2,1)S(1)}, bf16[8,768,512]{2,1,0:T(8,128)(2,1)}, u32[]{:S(2)}) copy-start(bf16[8,768,512]{2,1,0:T(8,128)(2,1)} %gather_fusion) | copy-start | bytes 18874372
  93.0 12.7 %copy-start.12 = (f32[4096]{0:T(1024)S(1)}, f32[4096]{0:T(1024)}, u32[]{:S(2)}) copy-start(f32[4096]{0:T(1024)} %param.12) | copy-start | bytes 49156
  119.2 12.5 %slice-start.3 = ((s8[6291456]{0:T(1024)(128)(4,1)}), s8[2097152]{0:T(1024)(128)(4,1)S(1)}, s32[]{:S(2)}) async-start(s8[6291456]{0:T(1024)(128)(4,1)} %bitcast.101), calls=%async_computation.7 | async-start | bytes 4194304
  122.0 9.7 %slice-start.4 = ((s8[6291456]{0:T(1024)(128)(4,1)}), s8[4194304]{0:T(1024)(128)(4,1)S(1)}, s32[]{:S(2)}) async-start(s8[6291456]{0:T(1024)(128)(4,1)} %bitcast.101), calls=%async_computation.8 | async-start | bytes 8388608
  122.0 9.7 %copy-start.6 = (bf16[128,4096]{1,0:T(8,128)(2,1)S(1)}, bf16[128,4096]{1,0:T(8,128)(2,1)}, u32[]{:S(2)}) copy-start(bf16[128,4096]{1,0:T(8,128)(2,1)} %copy.63) | copy-start | bytes 3145732
  122.0 10.8 %copy-start.3 = (bf16[256,4096]{1,0:T(8,128)(2,1)S(1)}, bf16[256,4096]{1,0:T(8,128)(2,1)}, u32[]{:S(2)}) copy-start(bf16[256,4096]{1,0:T(8,128)(2,1)} %copy.70) | copy-start | bytes 6291460
  127.1 4.6 %copy-start.10 = (bf16[768,128]{1,0:T(8,128)(2,1)}, bf16[768,128]{1,0:T(8,128)(2,1)S(1)}, u32[]{:S(2)}) copy-start(bf16[768,128]{1,0:T(8,128)(2,1)S(1)} %convolution_convert_fusion.1) | copy-start | bytes 589828
  127.1 18.8 %collective-permute-start.7 = (bf16[8,128]{1,0:T(8,128)(2,1)S(1)}, bf16[8,128]{1,0:T(8,128)(2,1)S(1)}, u32[]{:S(2)}, u32[]{:S(2)}) collective-permute-start(bf16[8,128]{1,0:T(8,128)(2,1)S(1)} %get-tuple-element.22), channel_id=1, source_target_pairs={{0,8},{8,16},{16,24},{24,32},{32,40},{40,48},{48,56},{56,64},{64,7... | collective-permute-start | bytes 6152 | tf_op jit(solution)/shard_map/ppermute | solution.py:27
  130.2 15.7 %collective-permute-start.8 = (bf16[8,128]{1,0:T(8,128)(2,1)S(1)}, bf16[8,128]{1,0:T(8,128)(2,1)S(1)}, u32[]{:S(2)}, u32[]{:S(2)}) collective-permute-start(bf16[8,128]{1,0:T(8,128)(2,1)S(1)} %get-tuple-element.23), channel_id=1, source_target_pairs={{8,0},{16,8},{24,16},{32,24},{40,32},{48,40},{56,48},{64,56},{72,6... | collective-permute-start | bytes 6152 | tf_op jit(solution)/shard_map/ppermute | solution.py:30
  132.8 2.8 %slice-start.5 = ((s8[6291456]{0:T(1024)(128)(4,1)}), s8[4194304]{0:T(1024)(128)(4,1)S(1)}, s32[]{:S(2)}) async-start(s8[6291456]{0:T(1024)(128)(4,1)} %bitcast.105), calls=%async_computation.9 | async-start | bytes 8388608
  132.8 2.3 copy-start.4
  132.9 3.0 %slice-start.6 = ((s8[6291456]{0:T(1024)(128)(4,1)}), s8[2097152]{0:T(1024)(128)(4,1)S(1)}, s32[]{:S(2)}) async-start(s8[6291456]{0:T(1024)(128)(4,1)} %bitcast.105), calls=%async_computation.10 | async-start | bytes 4194304
  135.2 10.7 %copy-start.11 = (bf16[768,128]{1,0:T(8,128)(2,1)S(1)}, bf16[768,128]{1,0:T(8,128)(2,1)}, u32[]{:S(2)}) copy-start(bf16[768,128]{1,0:T(8,128)(2,1)} %copy-done.10) | copy-start | bytes 589828
  138.2 7.9 %copy-start.8 = (bf16[768,128]{0,1:T(8,128)(2,1)}, bf16[768,128]{0,1:T(8,128)(2,1)S(1)}, u32[]{:S(2)}) copy-start(bf16[768,128]{0,1:T(8,128)(2,1)S(1)} %convolution_convert_fusion) | copy-start | bytes 589828
  139.4 41.9 %collective-permute-start.10 = (bf16[128,256]{0,1:T(8,128)(2,1)}, bf16[128,256]{0,1:T(8,128)(2,1)}, u32[]{:S(2)}, u32[]{:S(2)}) collective-permute-start(bf16[128,256]{0,1:T(8,128)(2,1)} %get-tuple-element.17), channel_id=1, source_target_pairs={{8,0},{16,8},{24,16},{32,24},{40,32},{48,40},{56,48},{64,56},{72,6... | collective-permute-start | bytes 196616 | tf_op jit(solution)/shard_map/ppermute | solution.py:30
  140.7 40.6 %collective-permute-start.9 = (bf16[128,256]{0,1:T(8,128)(2,1)S(1)}, bf16[128,256]{0,1:T(8,128)(2,1)}, u32[]{:S(2)}, u32[]{:S(2)}) collective-permute-start(bf16[128,256]{0,1:T(8,128)(2,1)S(1)} %get-tuple-element.16), channel_id=1, source_target_pairs={{0,8},{8,16},{16,24},{24,32},{32,40},{40,48},{48,56},{56,64},{64,7... | collective-permute-start | bytes 196616 | tf_op jit(solution)/shard_map/ppermute | solution.py:27
  173.6 7.7 %copy-start.9 = (bf16[768,128]{0,1:T(8,128)(2,1)S(1)}, bf16[768,128]{0,1:T(8,128)(2,1)}, u32[]{:S(2)}) copy-start(bf16[768,128]{0,1:T(8,128)(2,1)} %copy-done.8) | copy-start | bytes 589828
  188.0 4.2 %slice-start = ((s8[12582912]{0:T(1024)(128)(4,1)}), s8[4194304]{0:T(1024)(128)(4,1)S(1)}, s32[]{:S(2)}) async-start(s8[12582912]{0:T(1024)(128)(4,1)} %bitcast.99), calls=%async_computation.4 | async-start | bytes 8388608
  188.0 4.9 %slice-start.1 = ((s8[12582912]{0:T(1024)(128)(4,1)}), s8[4194304]{0:T(1024)(128)(4,1)S(1)}, s32[]{:S(2)}) async-start(s8[12582912]{0:T(1024)(128)(4,1)} %bitcast.99), calls=%async_computation.5 | async-start | bytes 8388608
  188.0 6.1 %slice-start.2 = ((s8[12582912]{0:T(1024)(128)(4,1)}), s8[4194304]{0:T(1024)(128)(4,1)S(1)}, s32[]{:S(2)}) async-start(s8[12582912]{0:T(1024)(128)(4,1)} %bitcast.99), calls=%async_computation.6 | async-start | bytes 8388608
  188.0 7.0 %copy-start.2 = (bf16[384,4096]{1,0:T(8,128)(2,1)S(1)}, bf16[384,4096]{1,0:T(8,128)(2,1)}, u32[]{:S(2)}) copy-start(bf16[384,4096]{1,0:T(8,128)(2,1)} %all-gather.5.cloned.1.call-done) | copy-start | bytes 9437188
  (4 other events, 8.3 us)
Sparse Core Ops, SparseCore 0:
  9.9 85.4 all-gather.2
  97.9 75.7 all-gather.4
  199.7 47.3 reduce-scatter.1
